TPU v7x, 32 devices: a whole 2x2x4 slice. The times are simulated.
32 devices in a mesh: fs: 16 (over z, y, x), tp: 2 (over core).
Axes of the slice: x: 2, y: 2, z: 4, core: 2. Of those that a mesh axis runs over, the one named last changes fastest.
Arguments:
- inputs: bfloat16 [8192, 2048], P('fs', 'tp'), may hold values from -6 to 6
- value_cotangent: bfloat16 [8192, 2048], P('fs', 'tp'), may hold values from -6 to 6
- first_map: bfloat16 [8192, 2048], P('fs', 'tp'), may hold values from -6 to 6
- second_map: bfloat16 [8192, 2048], P('fs', 'tp'), may hold values from -6 to 6
- lambdas: float32 [16], P('tp'), may hold values from 0.3 to 0.8
- head_gain: float32 [128], replicated, may hold values from 0.1 to 1.9
- output_cotangent: bfloat16 [8192, 2048], P('fs', 'tp'), may hold values from -6 to 6
- value_factor: bfloat16 [2048, 256], replicated, may hold values from -0.125 to 0.125
- output_factor: bfloat16 [2048, 256], replicated, may hold values from -0.125 to 0.125
- value_weight: float32 [2048, 2048], P('fs', 'tp'), may hold values from -0.125 to 0.125
- output_weight: float32 [2048, 2048], P('tp', 'fs'), may hold values from -0.125 to 0.125
- value_moment: float32 [256, 2048], P('fs', 'tp'), may hold values from -6 to 6
- value_second: float32 [256, 2048], P('fs', 'tp'), may hold values from 0.25 to 4
- output_moment: float32 [256, 2048], P('fs', 'tp'), may hold values from -6 to 6
- output_second: float32 [256, 2048], P('fs', 'tp'), may hold values from 0.25 to 4
Outputs:
- value_master: float32 [2048, 2048], P('fs', 'tp')
- output_master: float32 [2048, 2048], P('tp', 'fs')
- value_moment_new: float32 [256, 2048], P('fs', 'tp')
- value_second_new: float32 [256, 2048], P('fs', 'tp')
- output_moment_new: float32 [256, 2048], P('fs', 'tp')
- output_second_new: float32 [256, 2048], P('fs', 'tp')
- value_copy: bfloat16 [2048, 2048], P(None, 'tp')
- output_copy: bfloat16 [2048, 2048], P('tp')
All inputs are finite; a program needn't handle non-finite values.
Results may differ from a plain program's by a relative error of at most 0.0027.
Values may be sent and summed in bfloat16 or wider, within the bound.
A program may use at most 64 MiB of HBM per device.

v0:
```python
import math

import jax
import jax.numpy as jnp
from jax import lax
from jax.sharding import PartitionSpec as P


def contract_rows(left, right, precise):
    if precise:
        return lax.dot_general(
            left,
            right,
            (((0,), (0,)), ((), ())),
            precision=lax.Precision.HIGHEST,
            preferred_element_type=jnp.float32,
        )
    return lax.dot_general(
        left, right, (((0,), (0,)), ((), ())), preferred_element_type=jnp.float32
    )


def local(
    inputs,
    value_cotangent,
    first_map,
    second_map,
    lambdas,
    head_gain,
    output_cotangent,
    value_factor,
    output_factor,
    value_weight,
    output_weight,
    value_moment,
    value_second,
    output_moment,
    output_second,
):
    tok_rows = inputs.shape[0]
    local_heads = lambdas.shape[0]
    head_width = head_gain.shape[0]
    head_cols = local_heads * head_width
    first = first_map.astype(jnp.float32).reshape(tok_rows, local_heads, head_width)
    second = second_map.astype(jnp.float32).reshape(tok_rows, local_heads, head_width)
    difference = first - lambdas[None, :, None] * second
    normed = (
        difference
        * lax.rsqrt(jnp.mean(difference * difference, axis=-1, keepdims=True) + 1e-06)
        * head_gain
    )
    heads_out = normed.reshape(tok_rows, head_cols).astype(jnp.bfloat16)
    full_inputs, full_cotangent = (
        lax.all_gather(inputs, "tp", axis=1, tiled=True),
        lax.all_gather(output_cotangent, "tp", axis=1, tiled=True),
    )
    token_scale = 1.0 / math.sqrt(tok_rows * lax.axis_size("fs"))
    fs_index = lax.axis_index("fs")
    width_rows = value_weight.shape[0]
    value_rows = lax.dynamic_slice_in_dim(
        value_factor, fs_index * width_rows, width_rows, 0
    ).astype(jnp.float32)
    output_rows = lax.dynamic_slice_in_dim(
        output_factor, fs_index * width_rows, width_rows, 0
    ).astype(jnp.float32)
    grad_value = contract_rows(full_inputs, value_cotangent, False) * token_scale
    grad_output = contract_rows(full_cotangent, heads_out, False) * token_scale
    partial_value = jnp.concatenate(
        [
            contract_rows(value_factor.astype(jnp.float32), grad_value, True),
            contract_rows(output_factor.astype(jnp.float32), grad_output, True),
        ],
        axis=1,
    )
    own_rows = lax.psum_scatter(partial_value, "fs", scatter_dimension=0, tiled=True)
    moments = jnp.concatenate([value_moment, output_moment], axis=1)
    seconds = jnp.concatenate([value_second, output_second], axis=1)
    moment_new = 0.8 * moments + 0.2 * own_rows
    second_new = 0.95 * seconds + 0.05 * own_rows * own_rows
    direction = moment_new / (jnp.sqrt(second_new) + 1e-08)
    full_direction = lax.all_gather(direction, "fs", axis=0, tiled=True)
    step_value = jnp.dot(
        value_rows,
        full_direction[:, :head_cols],
        precision=lax.Precision.HIGHEST,
        preferred_element_type=jnp.float32,
    )
    step_output = jnp.dot(
        output_rows,
        full_direction[:, head_cols:],
        precision=lax.Precision.HIGHEST,
        preferred_element_type=jnp.float32,
    )
    value_master = value_weight - 0.05 * step_value
    output_master = output_weight - 0.05 * step_output.T
    value_copy, output_copy = (
        lax.all_gather(value_master.astype(jnp.bfloat16), "fs", axis=0, tiled=True),
        lax.all_gather(output_master.astype(jnp.bfloat16), "fs", axis=1, tiled=True),
    )
    return (
        value_master,
        output_master,
        moment_new[:, :head_cols],
        second_new[:, :head_cols],
        moment_new[:, head_cols:],
        second_new[:, head_cols:],
        value_copy,
        output_copy,
    )


def solution(mesh):
    in_specs = (
        P("fs", "tp"),
        P("fs", "tp"),
        P("fs", "tp"),
        P("fs", "tp"),
        P("tp"),
        P(),
        P("fs", "tp"),
        P(),
        P(),
        P("fs", "tp"),
        P("tp", "fs"),
        P("fs", "tp"),
        P("fs", "tp"),
        P("fs", "tp"),
        P("fs", "tp"),
    )
    out_specs = (
        P("fs", "tp"),
        P("tp", "fs"),
        P("fs", "tp"),
        P("fs", "tp"),
        P("fs", "tp"),
        P("fs", "tp"),
        P(None, "tp"),
        P("tp", None),
    )
    return jax.shard_map(local, mesh=mesh, in_specs=in_specs, out_specs=out_specs, check_vma=False)
```

profile of v0, /device:TPU:0, one launch (start us, length us, event | category | flops | bytes accessed | tf_op | source)
XLA Modules:
  0.0 374.0 jit_solution(844891537116236253)
XLA Ops:
  7.2 0.0 copy-start
  7.2 0.0 all-gather.8.cloned.1.call-start
  7.2 0.7 all-gather.8.cloned.1.call-update
  7.9 0.0 all-gather.6.cloned.1.call-start
  8.0 0.7 all-gather.6.cloned.1.call-update
  8.7 0.0 reduce-scatter.4.cloned.1.call-start
  8.7 0.2 convert_bitcast_fusion
  9.0 0.0 copy-start.2
  9.0 0.5 copy.52
  9.5 0.7 copy-done.2
  10.2 0.2 convert_bitcast_fusion.1
  10.5 0.0 copy-start.15
  10.5 0.5 copy.51
  11.0 0.2 copy-done.15
  11.1 0.3 fusion.9
  11.4 0.6 multiply_reduce_fusion
  12.0 0.1 copy.44
  12.2 0.1 copy.45
  12.3 0.1 broadcast_bitcast_fusion
  12.4 10.5 %all-gather.8.cloned.1.call-done = bf16[512,2048]{1,0:T(8,128)(2,1)} async-done(((bf16[512,1024]{1,0:T(8,128)(2,1)}), bf16[512,2048]{1,0:T(8,128)(2,1)}) %all-gather.8.cloned.1.call-update) | async-done | bytes 2097168 | tf_op jit(solution)/shard_map/all_gather | solution.py:55
  22.9 0.6 mul.105
  23.5 1.0 copy-done.5
  24.5 2.8 fusion.18
  27.3 4.0 %fusion.13 = f32[256,1024]{0,1:T(8,128)S(1)} fusion(bf16[2048,256]{1,0:T(8,128)(2,1)S(1)} %copy-done.8, f32[1024,2048]{1,0:T(8,128)S(1)} %fusion.18), kind=kOutput, calls=%fused_computation.18 | convolution fusion | flops 6444548096 | bytes 10485760 | tf_op jit(solution)/shard_map/dot_general | solution.py:11
  31.4 0.0 copy-start.7
  31.4 4.8 %all-gather.6.cloned.1.call-done = bf16[512,2048]{1,0:T(8,128)(2,1)} async-done(((bf16[512,1024]{1,0:T(8,128)(2,1)}), bf16[512,2048]{1,0:T(8,128)(2,1)}) %all-gather.6.cloned.1.call-update) | async-done | bytes 2097168 | tf_op jit(solution)/shard_map/all_gather | solution.py:54
  36.2 4.0 %fusion.38 = f32[2048,1024]{1,0:T(8,128)S(1)} fusion(bf16[512,2048]{1,0:T(8,128)(2,1)} %all-gather.6.cloned.1.call-done, bf16[512,1024]{1,0:T(8,128)(2,1)S(1)} %copy-done), kind=kOutput, calls=%fused_computation.47 | convolution fusion | flops 2147483648 | bytes 11534336 | tf_op jit(solution)/shard_map/dot_general | solution.py:18
  40.2 6.9 %fusion.10 = f32[256,1024]{0,1:T(8,128)S(1)} fusion(bf16[2048,256]{1,0:T(8,128)(2,1)S(1)} %copy-done.7, f32[2048,1024]{1,0:T(8,128)S(1)} %fusion.38), kind=kOutput, calls=%fused_computation.17 | convolution fusion | flops 6444548096 | bytes 10485760 | tf_op jit(solution)/shard_map/dot_general | solution.py:11
  47.2 0.1 pad_maximum_fusion
  47.3 1.8 copy.49
  49.2 0.0 reduce-scatter.4.cloned.1.call-update
  49.2 0.0 all-gather.10.cloned.1.call-start
  49.3 82.7 %reduce-scatter.4.cloned.1.call-done = f32[16,2048]{1,0:T(8,128)} async-done(((f32[256,2048]{1,0:T(8,128)}), f32[16,2048]{1,0:T(8,128)}) %reduce-scatter.4.cloned.1.call-update) | async-done | bytes 131088 | tf_op jit(solution)/shard_map/reduce_scatter | solution.py:75
  132.0 1.6 add_divide_fusion
  133.7 0.0 all-gather.10.cloned.1.call-update
  133.7 0.0 all-gather.12.cloned.1.call-start
  133.7 58.5 %all-gather.10.cloned.1.call-done = f32[256,2048]{1,0:T(8,128)} async-done(((f32[16,2048]{1,0:T(8,128)}), f32[256,2048]{1,0:T(8,128)}) %all-gather.10.cloned.1.call-update) | async-done | bytes 2097168 | tf_op jit(solution)/shard_map/all_gather | solution.py:81
  192.2 2.8 fusion.36
  195.0 0.0 all-gather.12.cloned.1.call-update
  195.0 0.0 all-gather.14.cloned.1.call-start
  195.1 2.7 fusion.37
  197.8 0.0 all-gather.14.cloned.1.call-update
  197.8 0.7 fusion.35
  198.5 0.7 fusion.34
  199.1 70.7 %all-gather.12.cloned.1.call-done = bf16[2048,1024]{1,0:T(8,128)(2,1)} async-done(((bf16[128,1024]{1,0:T(8,128)(2,1)}), bf16[2048,1024]{1,0:T(8,128)(2,1)}) %all-gather.12.cloned.1.call-update) | async-done | bytes 4194320 | tf_op jit(solution)/shard_map/all_gather | solution.py:97
  269.8 90.5 %all-gather.14.cloned.1.call-done = bf16[1024,2048]{1,0:T(8,128)(2,1)} async-done(((bf16[1024,128]{1,0:T(8,128)(2,1)}), bf16[1024,2048]{1,0:T(8,128)(2,1)}) %all-gather.14.cloned.1.call-update) | async-done | bytes 4194320 | tf_op jit(solution)/shard_map/all_gather | solution.py:98
  360.3 4.8 %copy.58 = bf16[2048,1024]{1,0:T(8,128)(2,1)} copy(bf16[2048,1024]{1,0:T(8,128)(2,1)} %all-gather.12.cloned.1.call-done) | data formatting | bytes 8388608
  365.1 2.0 copy.59
  (28 shorter events, 0.1 us)
Async XLA Ops:
  7.2 29.0 %copy-start = (bf16[512,1024]{1,0:T(8,128)(2,1)S(1)}, bf16[512,1024]{1,0:T(8,128)(2,1)}, u32[]{:S(2)}) copy-start(bf16[512,1024]{1,0:T(8,128)(2,1)} %param.16) | copy-start | bytes 3145732
  7.2 1.5 copy-start.3
  7.2 15.7 %all-gather.8.cloned.1.call-start = ((), (), s32[]{:S(2)}) async-start(), calls=%async_computation.2 | async-start | bytes 3145728 | tf_op jit(solution)/shard_map/all_gather | solution.py:55
  7.9 28.3 %all-gather.6.cloned.1.call-start = ((), (), s32[]{:S(2)}) async-start(), calls=%async_computation.1 | async-start | bytes 3145728 | tf_op jit(solution)/shard_map/all_gather | solution.py:54
  8.7 123.3 %reduce-scatter.4.cloned.1.call-start = ((), (), s32[]{:S(2)}) async-start(), calls=%async_computation.6 | async-start | bytes 2228224 | tf_op jit(solution)/shard_map/reduce_scatter | solution.py:75
  9.0 1.2 copy-start.2
  10.5 0.7 copy-start.15
  11.4 0.9 copy-start.16
  22.9 1.6 copy-start.5
  24.5 2.8 copy-start.8
  31.4 8.9 %copy-start.7 = (bf16[2048,256]{1,0:T(8,128)(2,1)S(1)}, bf16[2048,256]{1,0:T(8,128)(2,1)}, u32[]{:S(2)}) copy-start(bf16[2048,256]{1,0:T(8,128)(2,1)} %param.22) | copy-start | bytes 3145732
  49.1 82.9 %copy-start.11 = (f32[16,1024]{1,0:T(8,128)S(1)}, f32[16,1024]{1,0:T(8,128)}, u32[]{:S(2)}) copy-start(f32[16,1024]{1,0:T(8,128)} %param.29) | copy-start | bytes 196612
  49.1 82.9 %copy-start.12 = (f32[16,1024]{1,0:T(8,128)S(1)}, f32[16,1024]{1,0:T(8,128)}, u32[]{:S(2)}) copy-start(f32[16,1024]{1,0:T(8,128)} %param.27) | copy-start | bytes 196612
  49.1 82.9 %copy-start.13 = (f32[16,1024]{1,0:T(8,128)S(1)}, f32[16,1024]{1,0:T(8,128)}, u32[]{:S(2)}) copy-start(f32[16,1024]{1,0:T(8,128)} %param.28) | copy-start | bytes 196612
  49.1 82.9 %copy-start.14 = (f32[16,1024]{1,0:T(8,128)S(1)}, f32[16,1024]{1,0:T(8,128)}, u32[]{:S(2)}) copy-start(f32[16,1024]{1,0:T(8,128)} %param.26) | copy-start | bytes 196612
  49.2 143.0 %copy-start.9 = (f32[128,1024]{1,0:T(8,128)S(1)}, f32[128,1024]{1,0:T(8,128)}, u32[]{:S(2)}) copy-start(f32[128,1024]{1,0:T(8,128)} %param.24) | copy-start | bytes 1572868
  49.2 145.9 %copy-start.10 = (f32[1024,128]{1,0:T(8,128)S(1)}, f32[1024,128]{1,0:T(8,128)}, u32[]{:S(2)}) copy-start(f32[1024,128]{1,0:T(8,128)} %param.25) | copy-start | bytes 1572868
  49.2 143.0 %all-gather.10.cloned.1.call-start = ((), (), s32[]{:S(2)}) async-start(), calls=%async_computation.3 | async-start | bytes 2228224 | tf_op jit(solution)/shard_map/all_gather | solution.py:81
  133.7 136.1 %all-gather.12.cloned.1.call-start = ((), (), s32[]{:S(2)}) async-start(), calls=%async_computation.4 | async-start | bytes 4456448 | tf_op jit(solution)/shard_map/all_gather | solution.py:97
  192.2 2.9 copy-start.6
  195.0 165.3 %all-gather.14.cloned.1.call-start = ((), (), s32[]{:S(2)}) async-start(), calls=%async_computation.5 | async-start | bytes 4456448 | tf_op jit(solution)/shard_map/all_gather | solution.py:98
  360.3 4.8 %copy-start.4 = (bf16[1024,2048]{1,0:T(8,128)(2,1)S(1)}, bf16[1024,2048]{1,0:T(8,128)(2,1)}, u32[]{:S(2)}) copy-start(bf16[1024,2048]{1,0:T(8,128)(2,1)} %all-gather.14.cloned.1.call-done) | copy-start | bytes 12582916
  365.1 2.0 copy-start.1
Sparse Core Ops, SparseCore 0:
  9.5 13.2 all-gather.7
  24.4 11.7 all-gather.5
  49.3 82.6 reduce-scatter.3
  135.2 56.9 all-gather.9
  195.4 74.3 all-gather.11
  272.9 87.3 all-gather.13
where the time goes:
time: 374 us
  waiting for transfers between devices  319 us (85%)
  matrix products  23.3 us (6%)
  between operations  14.3 us (4%)
  local copies, waits for them, and re-layouts  13.8 us (4%)
    all_gather x1, waiting for transfers between devices, local(): lax.all_gather(output_master.astype(jnp.bfloat16), 'fs', axis=1, tiled=True)  90.5 us
    reduce_scatter x1, waiting for transfers between devices, local(): lax.psum_scatter(partial_value, 'fs', scatter_dimension=0, tiled=True)  82.7 us
    all_gather x1, waiting for transfers between devices, local(): lax.all_gather(value_master.astype(jnp.bfloat16), 'fs', axis=0, tiled=True)  70.7 us
    all_gather x1, waiting for transfers between devices, local(): full_direction = lax.all_gather(direction, 'fs', axis=0, tiled=True)  58.5 us
    unnamed x39, local copies, waits for them, and re-layouts  11.6 us
    dot_general x2, matrix products, contract_rows(): lax.dot_general(left, right, (((0,), (0,)), ((), ())), precision=lax.Prec...  10.9 us
    all_gather x1, waiting for transfers between devices, local(): lax.all_gather(output_cotangent, 'tp', axis=1, tiled=True)  10.5 us
  transfers between devices with their start and end apart: 6, of which 6 were waited for; matrix products, arithmetic and copies ran while one was open for 4% of the time, Pallas kernels for 0%

commit v1 on v0

v1 whole, which is shorter than its diff:
```python
import functools
import math

import jax
import jax.numpy as jnp
from jax import lax
from jax.experimental import pallas as pl
from jax.experimental.pallas import tpu as pltpu
from jax.sharding import PartitionSpec as P

F32 = jnp.float32
BF16 = jnp.bfloat16


CODE = 2.0**30


def encode(w):
    square = (w * CODE) * (w * CODE)
    fourth = square * square
    return jnp.where(w < 0, -fourth, fourth).astype(BF16)


def decode(v):
    v = v.astype(F32)
    size = lax.rsqrt(lax.rsqrt(jnp.abs(v))) * (1.0 / CODE)
    return jnp.where(v < 0, -size, size)


def exchange(
    nfs, ntp, scale,
    vw, ow, inp, vcot, first, second, ocot, lam, gain, vfac, ofac, vm, vs, om, os_,
    gv, go, dfull, vm_new, vs_new, om_new, os_new,
    heads, proj, part, got, direction,
    vsend, vrecv, osend, orecv, psend, precv, rsend, rrecv, dsend, drecv, lsem,
):
    me = lax.axis_index("fs")
    tp = lax.axis_index("tp")
    cols = inp.shape[1]
    rank = vfac.shape[1]
    nx = 2 if nfs % 2 == 0 else 1
    ny = 2 if nfs % 4 == 0 else 1
    nz = nfs // (nx * ny)
    x = lax.rem(me, nx)
    y = lax.rem(lax.div(me, nx), ny)
    z = lax.div(me, nx * ny)

    def at(dz, dy, dx):
        zz = lax.rem(z + dz, nz)
        yy = lax.rem(y + dy, ny)
        xx = lax.rem(x + dx, nx)
        return (zz * ny + yy) * nx + xx

    barrier = pltpu.get_barrier_semaphore()
    for k in range(1, nfs):
        pl.semaphore_signal(barrier, inc=1, device_id={"fs": lax.rem(me + k, nfs)})
    for k in range(1, ntp):
        pl.semaphore_signal(barrier, inc=1, device_id={"tp": lax.rem(tp + k, ntp)})
    pl.semaphore_wait(barrier, nfs + ntp - 2)

    width = vw.shape[0]

    def vslot(b):
        return gv.at[b]

    def oslot(b):
        if len(go.shape) == 2:
            return go.at[:, pl.ds(pl.multiple_of(b * width, width), width)]
        return go.at[b]

    pending = []
    counts = {"v": 0, "o": 0}

    def send(kind, src, b, target):
        k = counts[kind]
        counts[kind] = k + 1
        slot, ss, rs = (vslot, vsend, vrecv) if kind == "v" else (oslot, osend, orecv)
        copy = pltpu.make_async_remote_copy(
            src_ref=slot(b) if src is None else src,
            dst_ref=slot(b),
            send_sem=ss.at[k],
            recv_sem=rs.at[b],
            device_id={"fs": target},
        )
        copy.start()
        pending.append(copy)

    def arrived(kind, b):
        slot, ss, rs = (vslot, vsend, vrecv) if kind == "v" else (oslot, osend, orecv)
        pltpu.make_async_remote_copy(
            src_ref=slot(b), dst_ref=slot(b), send_sem=ss.at[0], recv_sem=rs.at[b],
            device_id={"fs": me},
        ).wait_recv()

    own_v = pltpu.make_async_copy(vw, vslot(me), lsem.at[0])
    own_o = pltpu.make_async_copy(ow, oslot(me), lsem.at[1])
    own_v.start()
    own_o.start()
    for dz in range(1, nz):
        send("v", vw, me, at(dz, 0, 0))
        send("o", ow, me, at(dz, 0, 0))
    if ny > 1:
        send("v", vw, me, at(0, 1, 0))
    if nx > 1:
        send("o", ow, me, at(0, 0, 1))
        send("v", vw, me, at(0, 0, 1))
    if ny > 1:
        send("o", ow, me, at(0, 1, 0))

    proj[0, :, :rank] = jnp.dot(inp[...], vfac[...], preferred_element_type=F32)
    proj[0, :, rank:] = jnp.dot(ocot[...], ofac[...], preferred_element_type=F32)
    pcopies = []
    for k in range(1, ntp):
        copy = pltpu.make_async_remote_copy(
            src_ref=proj.at[0], dst_ref=proj.at[k],
            send_sem=psend.at[k], recv_sem=precv.at[k],
            device_id={"tp": lax.rem(tp + k, ntp)},
        )
        copy.start()
        pcopies.append(copy)

    head_width = gain.shape[1]
    for h in range(cols // head_width):
        span = pl.ds(h * head_width, head_width)
        diff = first[:, span].astype(F32) - lam[h] * second[:, span].astype(F32)
        mean = jnp.mean(diff * diff, axis=-1, keepdims=True)
        heads[:, span] = (diff * lax.rsqrt(mean + 1e-06) * gain[...]).astype(BF16)

    for copy in pcopies:
        copy.wait()
    total = proj[0]
    for k in range(1, ntp):
        total = total + proj[k]
    high = total.astype(BF16)
    low = (total - high.astype(F32)).astype(BF16)

    def contract(a, b):
        return lax.dot_general(a, b, (((0,), (0,)), ((), ())), preferred_element_type=F32)

    rows = vm.shape[0]
    low_v = (contract(high[:, :rank], vcot[...]) + contract(low[:, :rank], vcot[...])) * scale
    part[:, :, :cols] = low_v.astype(BF16).reshape(nfs, rows, cols)
    low_o = (contract(high[:, rank:], heads[...]) + contract(low[:, rank:], heads[...])) * scale
    part[:, :, cols:] = low_o.astype(BF16).reshape(nfs, rows, cols)

    rcopies = []
    for k in range(1, nfs):
        peer = lax.rem(me + k, nfs)
        copy = pltpu.make_async_remote_copy(
            src_ref=part.at[peer], dst_ref=got.at[k],
            send_sem=rsend.at[k], recv_sem=rrecv.at[k],
            device_id={"fs": peer},
        )
        copy.start()
        rcopies.append(copy)

    for dz in range(1, nz):
        b = at(dz, 0, 0)
        arrived("v", b)
        if ny > 1:
            send("v", None, b, at(0, 1, 0))
        arrived("o", b)
        if nx > 1:
            send("o", None, b, at(0, 0, 1))
            send("v", None, b, at(0, 0, 1))
        if ny > 1:
            send("o", None, b, at(0, 1, 0))

    for copy in rcopies:
        copy.wait_recv()
    own = part[me].astype(F32)
    for k in range(1, nfs):
        own = own + got[k].astype(F32)
    for off, m_ref, s_ref, m_out, s_out in (
        (0, vm, vs, vm_new, vs_new),
        (cols, om, os_, om_new, os_new),
    ):
        g = own[:, off:off + cols]
        m = 0.8 * m_ref[...] + 0.2 * g
        s = 0.95 * s_ref[...] + 0.05 * g * g
        m_out[...] = m
        s_out[...] = s
        direction[:, off:off + cols] = (m / (jnp.sqrt(s) + 1e-08)).astype(BF16)
    own_d = pltpu.make_async_copy(direction, dfull.at[me], lsem.at[2])
    own_d.start()
    dcopies = []
    for k in range(1, nfs):
        copy = pltpu.make_async_remote_copy(
            src_ref=direction, dst_ref=dfull.at[me],
            send_sem=dsend.at[k], recv_sem=drecv.at[k],
            device_id={"fs": lax.rem(me + k, nfs)},
        )
        copy.start()
        dcopies.append(copy)

    for dz in range(nz):
        if ny > 1:
            b = at(dz, 1, 0)
            arrived("v", b)
            if nx > 1:
                send("v", None, b, at(0, 0, 1))
        if nx > 1:
            b = at(dz, 0, 1)
            arrived("o", b)
            if ny > 1:
                send("o", None, b, at(0, 1, 0))

    for dz in range(nz):
        for dy in range(ny):
            if nx > 1:
                arrived("v", at(dz, dy, 1))
        for dx in range(nx):
            if ny > 1:
                arrived("o", at(dz, 1, dx))
    for k, copy in enumerate(dcopies):
        src = lax.rem(me + nfs - (k + 1), nfs)
        pltpu.make_async_remote_copy(
            src_ref=direction, dst_ref=dfull.at[src],
            send_sem=dsend.at[0], recv_sem=drecv.at[k + 1], device_id={"fs": src},
        ).wait_recv()
    for copy in rcopies + dcopies + pending:
        copy.wait_send()
    own_v.wait()
    own_o.wait()
    own_d.wait()


def local(
    nfs, ntp,
    inputs, value_cotangent, first_map, second_map, lambdas, head_gain,
    output_cotangent, value_factor, output_factor, value_weight, output_weight,
    value_moment, value_second, output_moment, output_second,
):
    tokens, cols = inputs.shape
    width = value_weight.shape[0]
    rank = value_factor.shape[1]
    rows = value_moment.shape[0]
    tp = lax.axis_index("tp")
    fs = lax.axis_index("fs")
    vfac = lax.dynamic_slice_in_dim(value_factor, tp * cols, cols, 0)
    ofac = lax.dynamic_slice_in_dim(output_factor, tp * cols, cols, 0)
    scale = 1.0 / math.sqrt(tokens * nfs)
    flat = width % 128 == 0
    go_shape = (cols, nfs * width) if flat else (nfs, cols, width)
    vmem = pl.BlockSpec(memory_space=pltpu.VMEM)
    hbm = pl.BlockSpec(memory_space=pl.ANY)
    dma = pltpu.SemaphoreType.DMA
    moment = jax.ShapeDtypeStruct((rows, cols), F32)
    gv, go, dfull, vm_new, vs_new, om_new, os_new = pl.pallas_call(
        functools.partial(exchange, nfs, ntp, scale),
        out_shape=(
            jax.ShapeDtypeStruct((nfs, width, cols), BF16),
            jax.ShapeDtypeStruct(go_shape, BF16),
            jax.ShapeDtypeStruct((nfs, rows, 2 * cols), BF16),
            moment, moment, moment, moment,
        ),
        in_specs=[vmem] * 7 + [pl.BlockSpec(memory_space=pltpu.SMEM)] + [vmem] * 7,
        out_specs=(hbm, hbm, hbm, vmem, vmem, vmem, vmem),
        scratch_shapes=[
            pltpu.VMEM((tokens, cols), BF16),
            pltpu.VMEM((ntp, tokens, 2 * rank), F32),
            pltpu.VMEM((nfs, rows, 2 * cols), BF16),
            pltpu.VMEM((nfs, rows, 2 * cols), BF16),
            pltpu.VMEM((rows, 2 * cols), BF16),
            dma((nfs,)), dma((nfs,)), dma((nfs,)), dma((nfs,)),
            dma((ntp,)), dma((ntp,)),
            dma((nfs,)), dma((nfs,)), dma((nfs,)), dma((nfs,)), dma((3,)),
        ],
        compiler_params=pltpu.CompilerParams(collective_id=0, has_side_effects=True),
    )(
        encode(value_weight), encode(output_weight),
        inputs, value_cotangent, first_map, second_map, output_cotangent,
        lambdas, head_gain.reshape(1, -1), vfac, ofac,
        value_moment, value_second, output_moment, output_second,
    )
    dirs = dfull.reshape(nfs * rows, 2 * cols)
    dir_v, dir_o = dirs[:, :cols], dirs[:, cols:]
    vrows = lax.dynamic_slice_in_dim(value_factor, fs * width, width, 0)
    orows = lax.dynamic_slice_in_dim(output_factor, fs * width, width, 0)

    def step_v(factor):
        return jnp.dot(factor, dir_v, preferred_element_type=F32)

    def step_o(factor):
        return lax.dot_general(
            dir_o, factor, (((0,), (1,)), ((), ())), preferred_element_type=F32
        )

    value_master = value_weight - 0.05 * step_v(vrows)
    output_master = output_weight - 0.05 * step_o(orows)
    whole_v = decode(gv.reshape(nfs * width, cols))
    whole_o = decode(go if flat else go.transpose(1, 0, 2).reshape(cols, nfs * width))
    value_copy = (whole_v - 0.05 * step_v(value_factor)).astype(BF16)
    output_copy = (whole_o - 0.05 * step_o(output_factor)).astype(BF16)
    return (
        value_master, output_master, vm_new, vs_new, om_new, os_new,
        value_copy, output_copy,
    )


def solution(mesh):
    both = P("fs", "tp")
    in_specs = (
        both, both, both, both, P("tp"), P(), both, P(), P(), both, P("tp", "fs"),
        both, both, both, both,
    )
    out_specs = (
        both, P("tp", "fs"), both, both, both, both, P(None, "tp"), P("tp", None),
    )
    body = functools.partial(local, mesh.shape["fs"], mesh.shape["tp"])
    return jax.shard_map(
        body, mesh=mesh, in_specs=in_specs, out_specs=out_specs, check_vma=False
    )
```

time: 374 us -> 193 us (0.52)
  the two profiles are of different devices: /device:TPU:0 before, /device:TPU:8 now
where the time goes in v1:
time: 193 us
  Pallas kernels  139 us (72%)
  local copies, waits for them, and re-layouts  25.3 us (13%)
  matrix products  17.2 us (9%)
  other arithmetic  10.6 us (5%)
    pallas_call x1, Pallas kernels, local(): pl.pallas_call(functools.partial(exchange, nfs, ntp, scale), out_shape=(j...  139 us
    mul x1, local copies, waits for them, and re-layouts, decode(): size = lax.rsqrt(lax.rsqrt(jnp.abs(v))) * (1.0 / CODE)  9.16 us
    unnamed x25, local copies, waits for them, and re-layouts  8.99 us
    dot_general x2, matrix products, step_v(): return jnp.dot(factor, dir_v, preferred_element_type=F32)  8.92 us
    dot_general x2, matrix products, step_o(): lax.dot_general(dir_o, factor, (((0,), (1,)), ((), ())), preferred_elemen...  8.23 us
    mul x1, other arithmetic, decode(): size = lax.rsqrt(lax.rsqrt(jnp.abs(v))) * (1.0 / CODE)  5.41 us
    lt x1, local copies, waits for them, and re-layouts, decode(): return jnp.where(v < 0, -size, size)  4.87 us

profile of v1, /device:TPU:8, one launch (start us, length us, event | category | flops | bytes accessed | tf_op | source)
XLA Modules:
  0.0 192.6 jit_solution(4284173451131485604)
XLA Ops:
  0.6 0.0 copy-start.5
  0.7 1.9 %fusion.12.vw = bf16[128,1024]{1,0:T(8,128)(2,1)} fusion(f32[128,1024]{1,0:T(8,128)} %param.24), kind=kLoop, calls=%fused_computation.22 | loop fusion | flops 917504 | bytes 786432 | tf_op jit(solution)/shard_map/convert_element_type | solution.py:21
  2.6 1.9 fusion.13.ow
  4.5 2.2 %constant_dynamic-slice_fusion = (bf16[1024,256]{1,0:T(8,128)(2,1)}, bf16[1024,256]{1,0:T(8,128)(2,1)}) fusion(bf16[2048,256]{1,0:T(8,128)(2,1)} %param.23, s32[]{:T(128)S(6)} %select_n.27, bf16[2048,256]{1,0:T(8,128)(2,1)} %param.22), kind=kLoop, calls=%fused_computation.31 | loop fusion | bytes 2097156 | tf_op jit(solution)/shard_map/dynamic_slice | solution.py:241
  6.7 138.9 %shard_map.206 = (bf16[16,128,1024]{2,1,0:T(8,128)(2,1)}, bf16[1024,2048]{1,0:T(8,128)(2,1)}, bf16[16,16,2048]{2,1,0:T(8,128)(2,1)}, f32[16,1024]{1,0:T(8,128)},...) custom-call(bf16[128,1024]{1,0:T(8,128)(2,1)} %fusion.12.vw, bf16[1024,128]{1,0:T(8,128)(2,1)} %fusion.13.ow, ...), custom_call_target="tpu_custom_call" | custom-call | tf_op jit(solution)/shard_map/pallas_call | solution.py:249
  145.6 0.0 copy-done.5
  145.6 0.0 copy-start.2
  145.6 0.0 copy-start.3
  145.6 0.0 copy-start.1
  145.6 0.0 copy-start.4
  145.6 0.0 copy-start
  145.6 7.1 %fusion.9 = bf16[1024,2048]{1,0:T(8,128)(2,1)} fusion(bf16[1024,2048]{1,0:T(8,128)(2,1)} %get-tuple-element.21, bf16[2048,256]{1,0:T(8,128)(2,1)S(1)} %copy-done.5, bf16[256,2048]{1,0:T(8,128)(2,1)} %bitcast.10), kind=kOutput, calls=%fused_computation.15 | convolution fusion | flops 1092616192 | bytes 9961472 | tf_op jit(solution)/shard_map/dot_general | solution.py:285
  152.7 0.0 copy-done.2
  152.7 0.0 copy-done.3
  152.7 1.1 fusion.10
  153.9 0.0 copy-done.1
  153.9 0.0 copy-done.4
  153.9 1.0 fusion.11
  154.9 0.0 copy-done
  154.9 1.4 convert_compare_fusion.1
  156.3 4.9 %copy.26 = pred[2048,1024]{0,1:T(32,128)(4,1)S(1)} copy(pred[2048,1024]{1,0:T(32,128)(4,1)S(1)} %bitcast.9) | data formatting | bytes 4194304 | tf_op jit(solution)/shard_map/lt | solution.py:27
  161.1 5.4 %fusion.2 = f32[16,128,1024]{2,1,0:T(8,128)} fusion(bf16[16,128,1024]{2,1,0:T(8,128)(2,1)S(1)} %copy-done), kind=kLoop, calls=%fused_computation.8 | loop fusion | flops 6291456 | bytes 12582912 | tf_op jit(solution)/shard_map/mul | solution.py:26
  166.6 9.2 %copy.27 = f32[2048,1024]{0,1:T(8,128)} copy(f32[2048,1024]{1,0:T(8,128)} %bitcast.8) | data formatting | bytes 16777216 | tf_op jit(solution)/shard_map/mul | solution.py:26
  175.7 0.0 copy-start.9
  175.7 0.0 copy-start.8
  175.7 7.9 %fusion.7 = bf16[2048,1024]{0,1:T(8,128)(2,1)} fusion(pred[2048,1024]{0,1:T(32,128)(4,1)S(1)} %copy.26, f32[2048,1024]{0,1:T(8,128)} %copy.27, bf16[2048,256]{1,0:T(8,128)(2,1)S(1)} %copy-done.1, bf16[256,2048]{1,0:T(8,128)(2,1)} %bitcast.11), kind=kOutput, calls=%fused_computation.13 | convolution fusion | flops 1084227584 | bytes 16252928 | tf_op jit(solution)/shard_map/dot_general | solution.py:282
  183.6 0.0 copy-start.7
  183.6 0.0 copy-start.6
  183.6 6.4 %copy.25 = bf16[2048,1024]{1,0:T(8,128)(2,1)} copy(bf16[2048,1024]{0,1:T(8,128)(2,1)} %fusion.7) | data formatting | bytes 8388608
  190.0 0.0 copy-done.9
  190.0 0.6 copy.34
  190.7 0.0 copy-done.8
  190.7 0.6 copy.35
  191.3 0.0 copy-done.7
  191.3 0.6 copy.36
  191.9 0.0 copy-done.6
  191.9 0.6 copy.37
Async XLA Ops:
  0.6 144.9 %copy-start.5 = (bf16[2048,256]{1,0:T(8,128)(2,1)S(1)}, bf16[2048,256]{1,0:T(8,128)(2,1)}, u32[]{:S(2)}) copy-start(bf16[2048,256]{1,0:T(8,128)(2,1)} %param.23) | copy-start | bytes 3145732
  145.6 7.1 %copy-start.2 = (bf16[16,16,2048]{2,1,0:T(8,128)(2,1)S(1)}, bf16[16,16,2048]{2,1,0:T(8,128)(2,1)}, u32[]{:S(2)}) copy-start(bf16[16,16,2048]{2,1,0:T(8,128)(2,1)} %get-tuple-element.15) | copy-start | bytes 3145732
  145.6 7.1 %copy-start.3 = (f32[1024,128]{1,0:T(8,128)S(1)}, f32[1024,128]{1,0:T(8,128)}, u32[]{:S(2)}) copy-start(f32[1024,128]{1,0:T(8,128)} %param.25) | copy-start | bytes 1572868
  145.6 8.3 %copy-start.1 = (bf16[2048,256]{1,0:T(8,128)(2,1)S(1)}, bf16[2048,256]{1,0:T(8,128)(2,1)}, u32[]{:S(2)}) copy-start(bf16[2048,256]{1,0:T(8,128)(2,1)} %param.22) | copy-start | bytes 3145732
  145.6 8.3 %copy-start.4 = (f32[128,1024]{1,0:T(8,128)S(1)}, f32[128,1024]{1,0:T(8,128)}, u32[]{:S(2)}) copy-start(f32[128,1024]{1,0:T(8,128)} %param.24) | copy-start | bytes 1572868
  145.6 9.3 %copy-start = (bf16[16,128,1024]{2,1,0:T(8,128)(2,1)S(1)}, bf16[16,128,1024]{2,1,0:T(8,128)(2,1)}, u32[]{:S(2)}) copy-start(bf16[16,128,1024]{2,1,0:T(8,128)(2,1)} %get-tuple-element.20) | copy-start | bytes 12582916
  175.7 14.3 %copy-start.9 = (f32[16,1024]{1,0:T(8,128)S(1)}, f32[16,1024]{1,0:T(8,128)}, u32[]{:S(2)}) copy-start(f32[16,1024]{1,0:T(8,128)} %get-tuple-element.42) | copy-start | bytes 196612
  175.7 15.0 %copy-start.8 = (f32[16,1024]{1,0:T(8,128)S(1)}, f32[16,1024]{1,0:T(8,128)}, u32[]{:S(2)}) copy-start(f32[16,1024]{1,0:T(8,128)} %get-tuple-element.43) | copy-start | bytes 196612
  183.6 7.7 %copy-start.7 = (f32[16,1024]{1,0:T(8,128)S(1)}, f32[16,1024]{1,0:T(8,128)}, u32[]{:S(2)}) copy-start(f32[16,1024]{1,0:T(8,128)} %get-tuple-element.44) | copy-start | bytes 196612
  183.6 8.3 %copy-start.6 = (f32[16,1024]{1,0:T(8,128)S(1)}, f32[16,1024]{1,0:T(8,128)}, u32[]{:S(2)}) copy-start(f32[16,1024]{1,0:T(8,128)} %get-tuple-element.45) | copy-start | bytes 196612

commit v2 on v1

v2 whole, which is shorter than its diff:
```python
import functools
import math

import jax
import jax.numpy as jnp
from jax import lax
from jax.experimental import pallas as pl
from jax.experimental.pallas import tpu as pltpu
from jax.sharding import PartitionSpec as P

F32 = jnp.float32
BF16 = jnp.bfloat16


CODE = 2.0**30


def encode(w):
    square = (w * CODE) * (w * CODE)
    fourth = square * square
    return jnp.where(w < 0, -fourth, fourth).astype(BF16)


def decode(v):
    v = v.astype(F32)
    size = lax.rsqrt(lax.rsqrt(jnp.maximum(jnp.abs(v), 1e-36))) * (1.0 / CODE)
    return jnp.where(v < 0, -size, size)


def exchange(
    nfs, ntp, scale,
    vw, ow, inp, vcot, first, second, ocot, lam, gain, vfac, ofac, vm, vs, om, os_,
    gv, go, dfull, own_out,
    heads, proj, part, got, direction,
    vsend, vrecv, osend, orecv, psend, precv, rsend, rrecv,
    dvsend, dvrecv, dosend, dorecv, lsem,
):
    me = lax.axis_index("fs")
    tp = lax.axis_index("tp")
    cols = inp.shape[1]
    rank = vfac.shape[1]
    nx = 2 if nfs % 2 == 0 else 1
    ny = 2 if nfs % 4 == 0 else 1
    nz = nfs // (nx * ny)
    x = lax.rem(me, nx)
    y = lax.rem(lax.div(me, nx), ny)
    z = lax.div(me, nx * ny)

    def at(dz, dy, dx):
        zz = lax.rem(z + dz, nz)
        yy = lax.rem(y + dy, ny)
        xx = lax.rem(x + dx, nx)
        return (zz * ny + yy) * nx + xx

    barrier = pltpu.get_barrier_semaphore()
    for k in range(1, nfs):
        pl.semaphore_signal(barrier, inc=1, device_id={"fs": lax.rem(me + k, nfs)})
    for k in range(1, ntp):
        pl.semaphore_signal(barrier, inc=1, device_id={"tp": lax.rem(tp + k, ntp)})
    pl.semaphore_wait(barrier, nfs + ntp - 2)

    width = vw.shape[0]

    def vslot(b):
        return gv.at[b]

    def oslot(b):
        if len(go.shape) == 2:
            return go.at[:, pl.ds(pl.multiple_of(b * width, width), width)]
        return go.at[b]

    def dvslot(b):
        return dfull.at[b, :, pl.ds(0, cols)]

    def doslot(b):
        return dfull.at[b, :, pl.ds(cols, cols)]

    kinds = {
        "v": (vslot, vsend, vrecv),
        "o": (oslot, osend, orecv),
        "dv": (dvslot, dvsend, dvrecv),
        "do": (doslot, dosend, dorecv),
    }
    pending = []
    counts = {kind: 0 for kind in kinds}

    def when(cond, run):
        if cond is None:
            run()
        else:
            pl.when(cond)(run)

    def send(kind, src, b, target, cond=None):
        k = counts[kind]
        counts[kind] = k + 1
        slot, ss, rs = kinds[kind]

        def make():
            return pltpu.make_async_remote_copy(
                src_ref=slot(b) if src is None else src,
                dst_ref=slot(b),
                send_sem=ss.at[k],
                recv_sem=rs.at[b],
                device_id={"fs": target},
            )

        when(cond, lambda: make().start())
        pending.append((cond, make))

    def arrived(kind, b, cond=None):
        slot, ss, rs = kinds[kind]
        when(cond, lambda: pltpu.make_async_remote_copy(
            src_ref=slot(b), dst_ref=slot(b), send_sem=ss.at[0], recv_sem=rs.at[b],
            device_id={"fs": me},
        ).wait_recv())

    def spread(kind, src, b, cond=None):
        turns = ((ny, (0, 1, 0)), (nx, (0, 0, 1)))
        for extent, turn in turns if kind in ("v", "dv") else turns[::-1]:
            if extent > 1:
                send(kind, src, b, at(*turn), cond)

    def across(kind, bz, cond=None):
        first_turn, second_turn = (ny, nx) if kind in ("v", "dv") else (nx, ny)
        if first_turn == 1:
            return
        if kind in ("v", "dv"):
            b, target = (bz * ny + lax.rem(y + 1, ny)) * nx + x, at(0, 0, 1)
        else:
            b, target = (bz * ny + y) * nx + lax.rem(x + 1, nx), at(0, 1, 0)
        arrived(kind, b, cond)
        if second_turn > 1:
            send(kind, None, b, target, cond)

    def plane(bz):
        return (bz * ny + y) * nx + x

    up, down = lax.rem(z + 1, nz), lax.rem(z + nz - 1, nz)

    def along(kind, s):
        for sign in (1, -1):
            source = z - sign * s
            cond = source >= 0 if sign == 1 else source < nz
            b = plane(lax.rem(source + nz, nz))
            arrived(kind, b, cond)
            if sign == 1:
                send(kind, None, b, plane(up), (source >= 0) & (z + 1 < nz))
            else:
                send(kind, None, b, plane(down), (source < nz) & (z > 0))
            spread(kind, None, b, cond)

    def behind(kind, s):
        for sign in (1, -1):
            source = z - sign * s
            cond = source >= 0 if sign == 1 else source < nz
            across(kind, lax.rem(source + nz, nz), cond)

    own_v = pltpu.make_async_copy(vw, vslot(me), lsem.at[0])
    own_o = pltpu.make_async_copy(ow, oslot(me), lsem.at[1])
    own_v.start()
    own_o.start()
    for kind, src in (("v", vw), ("o", ow)):
        send(kind, src, me, plane(up), z + 1 < nz)
        send(kind, src, me, plane(down), z > 0)
        spread(kind, src, me)

    proj[0, :, :rank] = jnp.dot(inp[...], vfac[...], preferred_element_type=F32)
    proj[0, :, rank:] = jnp.dot(ocot[...], ofac[...], preferred_element_type=F32)
    pcopies = []
    for k in range(1, ntp):
        copy = pltpu.make_async_remote_copy(
            src_ref=proj.at[0], dst_ref=proj.at[k],
            send_sem=psend.at[k], recv_sem=precv.at[k],
            device_id={"tp": lax.rem(tp + k, ntp)},
        )
        copy.start()
        pcopies.append(copy)

    head_width = gain.shape[1]
    for h in range(cols // head_width):
        span = pl.ds(h * head_width, head_width)
        diff = first[:, span].astype(F32) - lam[h] * second[:, span].astype(F32)
        mean = jnp.mean(diff * diff, axis=-1, keepdims=True)
        heads[:, span] = (diff * lax.rsqrt(mean + 1e-06) * gain[...]).astype(BF16)

    for copy in pcopies:
        copy.wait()
    total = proj[0]
    for k in range(1, ntp):
        total = total + proj[k]
    high = total.astype(BF16)
    low = (total - high.astype(F32)).astype(BF16)

    def contract(a, b):
        return lax.dot_general(a, b, (((0,), (0,)), ((), ())), preferred_element_type=F32)

    rows = vm.shape[0]
    low_v = (contract(high[:, :rank], vcot[...]) + contract(low[:, :rank], vcot[...])) * scale
    part[:, :, :cols] = low_v.astype(BF16).reshape(nfs, rows, cols)
    low_o = (contract(high[:, rank:], heads[...]) + contract(low[:, rank:], heads[...])) * scale
    part[:, :, cols:] = low_o.astype(BF16).reshape(nfs, rows, cols)

    rcopies = []
    for k in range(1, nfs):
        peer = lax.rem(me + k, nfs)
        copy = pltpu.make_async_remote_copy(
            src_ref=part.at[peer], dst_ref=got.at[k],
            send_sem=rsend.at[k], recv_sem=rrecv.at[k],
            device_id={"fs": peer},
        )
        copy.start()
        rcopies.append(copy)

    for s in range(1, nz):
        for kind in ("v", "o"):
            along(kind, s)
        for kind in ("v", "o"):
            if s == 1:
                across(kind, z)
            else:
                behind(kind, s - 1)

    for copy in rcopies:
        copy.wait_recv()
    own = part[me].astype(F32)
    for k in range(1, nfs):
        own = own + got[k].astype(F32)
    own_out[...] = own
    for off, m_ref, s_ref in ((0, vm, vs), (cols, om, os_)):
        g = own[:, off:off + cols]
        m = 0.8 * m_ref[...] + 0.2 * g
        s = 0.95 * s_ref[...] + 0.05 * g * g
        direction[:, off:off + cols] = (m / (jnp.sqrt(s) + 1e-08)).astype(BF16)
    own_d = pltpu.make_async_copy(direction, dfull.at[me], lsem.at[2])
    own_d.start()
    halves = {"dv": direction.at[:, pl.ds(0, cols)], "do": direction.at[:, pl.ds(cols, cols)]}
    for kind, src in halves.items():
        for dz in range(1, nz):
            send(kind, src, me, at(dz, 0, 0))
        spread(kind, src, me)
    for dz in range(1, nz):
        for kind in halves:
            arrived(kind, at(dz, 0, 0))
            spread(kind, None, at(dz, 0, 0))
    for dz in range(nz):
        for kind in halves:
            across(kind, lax.rem(z + dz, nz))
    for kind in ("v", "o"):
        if nz > 1:
            behind(kind, nz - 1)
        else:
            across(kind, z)

    for dz in range(nz):
        for dy in range(ny):
            if nx > 1:
                arrived("v", at(dz, dy, 1))
                arrived("dv", at(dz, dy, 1))
        for dx in range(nx):
            if ny > 1:
                arrived("o", at(dz, 1, dx))
                arrived("do", at(dz, 1, dx))
    for copy in rcopies:
        copy.wait_send()
    for cond, make in pending:
        when(cond, lambda make=make: make().wait_send())
    own_v.wait()
    own_o.wait()
    own_d.wait()


def update(
    width, fs, gv, go, vfac, ofac, dv, do, vw, ow, own, vm, vs, om, os_,
    v_copy, o_copy, v_master, o_master, vm_new, vs_new, om_new, os_new, turned,
):
    step = pl.program_id(0)
    cols = dv.shape[1]

    @pl.when(step == 0)
    def _():
        turned[...] = do[...].T
        for off, m_ref, s_ref, m_out, s_out in (
            (0, vm, vs, vm_new, vs_new),
            (cols, om, os_, om_new, os_new),
        ):
            g = own[:, off:off + cols]
            m_out[...] = 0.8 * m_ref[...] + 0.2 * g
            s_out[...] = 0.95 * s_ref[...] + 0.05 * g * g

    move_v = 0.05 * jnp.dot(vfac[...], dv[...], preferred_element_type=F32)
    move_o = 0.05 * lax.dot_general(
        turned[...], ofac[...], (((1,), (1,)), ((), ())), preferred_element_type=F32
    )
    v_copy[...] = (decode(gv[0]) - move_v).astype(BF16)
    o_old = decode(go[...] if len(go.shape) == 2 else go[0])
    o_new = (o_old - move_o).astype(BF16)
    if len(go.shape) == 2:
        o_copy[...] = o_new
    else:
        o_copy[0] = o_new

    @pl.when(step == fs[0])
    def _():
        v_master[...] = vw[...] - move_v
        o_master[...] = ow[...] - move_o


def local(
    nfs, ntp,
    inputs, value_cotangent, first_map, second_map, lambdas, head_gain,
    output_cotangent, value_factor, output_factor, value_weight, output_weight,
    value_moment, value_second, output_moment, output_second,
):
    tokens, cols = inputs.shape
    width = value_weight.shape[0]
    rank = value_factor.shape[1]
    rows = value_moment.shape[0]
    tp = lax.axis_index("tp")
    fs = lax.axis_index("fs")
    vfac = lax.dynamic_slice_in_dim(value_factor, tp * cols, cols, 0)
    ofac = lax.dynamic_slice_in_dim(output_factor, tp * cols, cols, 0)
    scale = 1.0 / math.sqrt(tokens * nfs)
    flat = width % 128 == 0
    go_shape = (cols, nfs * width) if flat else (nfs, cols, width)
    vmem = pl.BlockSpec(memory_space=pltpu.VMEM)
    hbm = pl.BlockSpec(memory_space=pl.ANY)
    dma = pltpu.SemaphoreType.DMA
    moment = jax.ShapeDtypeStruct((rows, cols), F32)
    gv, go, dfull, own = pl.pallas_call(
        functools.partial(exchange, nfs, ntp, scale),
        out_shape=(
            jax.ShapeDtypeStruct((nfs, width, cols), BF16),
            jax.ShapeDtypeStruct(go_shape, BF16),
            jax.ShapeDtypeStruct((nfs, rows, 2 * cols), BF16),
            jax.ShapeDtypeStruct((rows, 2 * cols), F32),
        ),
        in_specs=[vmem] * 7 + [pl.BlockSpec(memory_space=pltpu.SMEM)] + [vmem] * 7,
        out_specs=(hbm, hbm, hbm, vmem),
        scratch_shapes=[
            pltpu.VMEM((tokens, cols), BF16),
            pltpu.VMEM((ntp, tokens, 2 * rank), F32),
            pltpu.VMEM((nfs, rows, 2 * cols), BF16),
            pltpu.VMEM((nfs, rows, 2 * cols), BF16),
            pltpu.VMEM((rows, 2 * cols), BF16),
            dma((2 * nfs + 1,)), dma((nfs,)), dma((2 * nfs + 1,)), dma((nfs,)),
            dma((ntp,)), dma((ntp,)),
            dma((nfs,)), dma((nfs,)),
            dma((nfs,)), dma((nfs,)), dma((nfs,)), dma((nfs,)), dma((3,)),
        ],
        compiler_params=pltpu.CompilerParams(collective_id=0, has_side_effects=True),
    )(
        encode(value_weight), encode(output_weight),
        inputs, value_cotangent, first_map, second_map, output_cotangent,
        lambdas, head_gain.reshape(1, -1), vfac, ofac,
        value_moment, value_second, output_moment, output_second,
    )
    dirs = dfull.reshape(nfs * rows, 2 * cols)
    same = lambda i: (0, 0)
    if flat:
        o_spec, oc_shape = pl.BlockSpec((cols, width), lambda i: (0, i)), (cols, nfs * width)
    else:
        o_spec, oc_shape = pl.BlockSpec((1, cols, width), lambda i: (i, 0, 0)), go_shape
    small = pl.BlockSpec((rows, cols), same)
    outs = pl.pallas_call(
        functools.partial(update, width),
        grid=(nfs,),
        out_shape=(
            jax.ShapeDtypeStruct((nfs * width, cols), BF16),
            jax.ShapeDtypeStruct(oc_shape, BF16),
            jax.ShapeDtypeStruct((width, cols), F32),
            jax.ShapeDtypeStruct((cols, width), F32),
            moment, moment, moment, moment,
        ),
        in_specs=[
            pl.BlockSpec(memory_space=pltpu.SMEM),
            pl.BlockSpec((1, width, cols), lambda i: (i, 0, 0)),
            o_spec,
            pl.BlockSpec((width, rank), lambda i: (i, 0)),
            pl.BlockSpec((width, rank), lambda i: (i, 0)),
            pl.BlockSpec((rank, cols), lambda i: (0, 0)),
            pl.BlockSpec((rank, cols), lambda i: (0, 1)),
            pl.BlockSpec((width, cols), same),
            pl.BlockSpec((cols, width), same),
            pl.BlockSpec((rows, 2 * cols), same),
            small, small, small, small,
        ],
        out_specs=(
            pl.BlockSpec((width, cols), lambda i: (i, 0)),
            o_spec,
            pl.BlockSpec((width, cols), same),
            pl.BlockSpec((cols, width), same),
            small, small, small, small,
        ),
        scratch_shapes=[pltpu.VMEM((cols, rank), BF16)],
        compiler_params=pltpu.CompilerParams(dimension_semantics=("arbitrary",)),
    )(
        fs.reshape(1), gv, go, value_factor, output_factor, dirs, dirs,
        value_weight, output_weight, own,
        value_moment, value_second, output_moment, output_second,
    )
    value_copy, output_copy, value_master, output_master, *moments = outs
    if not flat:
        output_copy = output_copy.transpose(1, 0, 2).reshape(cols, nfs * width)
    return (value_master, output_master, *moments, value_copy, output_copy)


def solution(mesh):
    both = P("fs", "tp")
    in_specs = (
        both, both, both, both, P("tp"), P(), both, P(), P(), both, P("tp", "fs"),
        both, both, both, both,
    )
    out_specs = (
        both, P("tp", "fs"), both, both, both, both, P(None, "tp"), P("tp", None),
    )
    body = functools.partial(local, mesh.shape["fs"], mesh.shape["tp"])
    return jax.shard_map(
        body, mesh=mesh, in_specs=in_specs, out_specs=out_specs, check_vma=False
    )
```

time: 193 us -> 126 us (0.65)
  the two profiles are of different devices: /device:TPU:8 before, /device:TPU:0 now
where the time goes in v2:
time: 126 us; the launch traced here: 125 us
  Pallas kernels  119 us (94%)
  other arithmetic  3.72 us (3%)
  local copies, waits for them, and re-layouts  2.23 us (2%)
    pallas_call x1, Pallas kernels, local(): pl.pallas_call(functools.partial(exchange, nfs, ntp, scale), out_shape=(j...  101 us
    pallas_call x1, Pallas kernels, local(): pl.pallas_call(functools.partial(update, width), grid=(nfs,), out_shape=(...  17.5 us
    convert_element_type x2, other arithmetic, encode(): return jnp.where(w < 0, -fourth, fourth).astype(BF16)  3.72 us

profile of v2, /device:TPU:0, one launch (start us, length us, event | category | flops | bytes accessed | tf_op | source)
XLA Modules:
  0.0 125.5 jit_solution(9597059106520214465)
XLA Ops:
  0.6 1.9 %fusion.vw = bf16[128,1024]{1,0:T(8,128)(2,1)} fusion(f32[128,1024]{1,0:T(8,128)} %vw.1), kind=kLoop, calls=%fused_computation.2 | loop fusion | flops 917504 | bytes 786432 | tf_op jit(solution)/shard_map/convert_element_type | solution.py:21
  2.5 1.9 %fusion.1.ow = bf16[1024,128]{1,0:T(8,128)(2,1)} fusion(f32[1024,128]{1,0:T(8,128)} %ow.1), kind=kLoop, calls=%fused_computation.3 | loop fusion | flops 917504 | bytes 786432 | tf_op jit(solution)/shard_map/convert_element_type | solution.py:21
  4.4 2.2 %constant_dynamic-slice_fusion = (bf16[1024,256]{1,0:T(8,128)(2,1)}, bf16[1024,256]{1,0:T(8,128)(2,1)}) fusion(bf16[2048,256]{1,0:T(8,128)(2,1)} %ofac.1, s32[]{:T(128)S(6)} %select_n.14, bf16[2048,256]{1,0:T(8,128)(2,1)} %vfac.1), kind=kLoop, calls=%fused_computation.4 | loop fusion | bytes 2097156 | tf_op jit(solution)/shard_map/dynamic_slice | solution.py:321
  6.6 101.4 %shard_map.206 = (bf16[16,128,1024]{2,1,0:T(8,128)(2,1)}, bf16[1024,2048]{1,0:T(8,128)(2,1)}, bf16[16,16,2048]{2,1,0:T(8,128)(2,1)}, f32[16,2048]{1,0:T(8,128)}) custom-call(bf16[128,1024]{1,0:T(8,128)(2,1)} %fusion.vw, bf16[1024,128]{1,0:T(8,128)(2,1)} %fusion.1.ow, bf16[512,1024]{1,0:T(8,128)(2,1)} %inp.1, bf16[512,1024]{1,0:T(8,128)(2,1)} %vcot.1, ...), custom_call_target="tpu_custom_call" | custom-call | tf_op jit(solution)/shard_map/pallas_call | solution.py:329
  108.0 17.5 %shard_map.207 = (bf16[2048,1024]{1,0:T(8,128)(2,1)}, bf16[1024,2048]{1,0:T(8,128)(2,1)}, f32[128,1024]{1,0:T(8,128)}, f32[1024,128]{1,0:T(8,128)}, f32[16,1024]...) custom-call(s32[1]{0:T(128)} %bitcast.fs, ...), custom_call_target="tpu_custom_call" | custom-call | tf_op jit(solution)/shard_map/pallas_call | solution.py:364

commit v3 on v2

--- a/solution.py
+++ b/solution.py
@@ -29,11 +29,12 @@
 
 def exchange(
     nfs, ntp, scale,
-    vw, ow, inp, vcot, first, second, ocot, lam, gain, vfac, ofac, vm, vs, om, os_,
+    vw_in, ow_in, inp_in, ocot_in, first_in, second_in, vcot_in, lam, gain, vfac, ofac,
+    vm, vs, om, os_,
     gv, go, dfull, own_out,
-    heads, proj, part, got, direction,
+    vw, ow, inp, ocot, first, second, vcot, heads, proj, part, got, direction,
     vsend, vrecv, osend, orecv, psend, precv, rsend, rrecv,
-    dvsend, dvrecv, dosend, dorecv, lsem,
+    dvsend, dvrecv, dosend, dorecv, lsem, insem,
 ):
     me = lax.axis_index("fs")
     tp = lax.axis_index("tp")
@@ -57,6 +58,14 @@
         pl.semaphore_signal(barrier, inc=1, device_id={"fs": lax.rem(me + k, nfs)})
     for k in range(1, ntp):
         pl.semaphore_signal(barrier, inc=1, device_id={"tp": lax.rem(tp + k, ntp)})
+    loads = []
+    pairs = ((inp_in, inp), (ocot_in, ocot), (first_in, first), (second_in, second), (vcot_in, vcot))
+    for k, (src, dst) in enumerate(pairs):
+        load = pltpu.make_async_copy(src, dst, insem.at[k])
+        load.start()
+        loads.append(load)
+    vw[...] = encode(vw_in[...])
+    ow[...] = encode(ow_in[...])
     pl.semaphore_wait(barrier, nfs + ntp - 2)
 
     width = vw.shape[0]
@@ -164,8 +173,11 @@
         send(kind, src, me, plane(down), z > 0)
         spread(kind, src, me)
 
-    proj[0, :, :rank] = jnp.dot(inp[...], vfac[...], preferred_element_type=F32)
-    proj[0, :, rank:] = jnp.dot(ocot[...], ofac[...], preferred_element_type=F32)
+    mine = pl.ds(pl.multiple_of(tp * cols, cols), cols)
+    loads[0].wait()
+    proj[0, :, :rank] = jnp.dot(inp[...], vfac[mine, :], preferred_element_type=F32)
+    loads[1].wait()
+    proj[0, :, rank:] = jnp.dot(ocot[...], ofac[mine, :], preferred_element_type=F32)
     pcopies = []
     for k in range(1, ntp):
         copy = pltpu.make_async_remote_copy(
@@ -176,6 +188,8 @@
         copy.start()
         pcopies.append(copy)
 
+    loads[2].wait()
+    loads[3].wait()
     head_width = gain.shape[1]
     for h in range(cols // head_width):
         span = pl.ds(h * head_width, head_width)
@@ -194,6 +208,7 @@
     def contract(a, b):
         return lax.dot_general(a, b, (((0,), (0,)), ((), ())), preferred_element_type=F32)
 
+    loads[4].wait()
     rows = vm.shape[0]
     low_v = (contract(high[:, :rank], vcot[...]) + contract(low[:, :rank], vcot[...])) * scale
     part[:, :, :cols] = low_v.astype(BF16).reshape(nfs, rows, cols)
@@ -315,10 +330,7 @@
     width = value_weight.shape[0]
     rank = value_factor.shape[1]
     rows = value_moment.shape[0]
-    tp = lax.axis_index("tp")
     fs = lax.axis_index("fs")
-    vfac = lax.dynamic_slice_in_dim(value_factor, tp * cols, cols, 0)
-    ofac = lax.dynamic_slice_in_dim(output_factor, tp * cols, cols, 0)
     scale = 1.0 / math.sqrt(tokens * nfs)
     flat = width % 128 == 0
     go_shape = (cols, nfs * width) if flat else (nfs, cols, width)
@@ -334,10 +346,12 @@
             jax.ShapeDtypeStruct((nfs, rows, 2 * cols), BF16),
             jax.ShapeDtypeStruct((rows, 2 * cols), F32),
         ),
-        in_specs=[vmem] * 7 + [pl.BlockSpec(memory_space=pltpu.SMEM)] + [vmem] * 7,
+        in_specs=[vmem] * 2 + [hbm] * 5 + [pl.BlockSpec(memory_space=pltpu.SMEM)] + [vmem] * 7,
         out_specs=(hbm, hbm, hbm, vmem),
         scratch_shapes=[
-            pltpu.VMEM((tokens, cols), BF16),
+            pltpu.VMEM((width, cols), BF16),
+            pltpu.VMEM((cols, width), BF16),
+            *[pltpu.VMEM((tokens, cols), BF16)] * 6,
             pltpu.VMEM((ntp, tokens, 2 * rank), F32),
             pltpu.VMEM((nfs, rows, 2 * cols), BF16),
             pltpu.VMEM((nfs, rows, 2 * cols), BF16),
@@ -345,13 +359,13 @@
             dma((2 * nfs + 1,)), dma((nfs,)), dma((2 * nfs + 1,)), dma((nfs,)),
             dma((ntp,)), dma((ntp,)),
             dma((nfs,)), dma((nfs,)),
-            dma((nfs,)), dma((nfs,)), dma((nfs,)), dma((nfs,)), dma((3,)),
+            dma((nfs,)), dma((nfs,)), dma((nfs,)), dma((nfs,)), dma((3,)), dma((5,)),
         ],
         compiler_params=pltpu.CompilerParams(collective_id=0, has_side_effects=True),
     )(
-        encode(value_weight), encode(output_weight),
-        inputs, value_cotangent, first_map, second_map, output_cotangent,
-        lambdas, head_gain.reshape(1, -1), vfac, ofac,
+        value_weight, output_weight,
+        inputs, output_cotangent, first_map, second_map, value_cotangent,
+        lambdas, head_gain.reshape(1, -1), value_factor, output_factor,
         value_moment, value_second, output_moment, output_second,
     )
     dirs = dfull.reshape(nfs * rows, 2 * cols)

time: 126 us -> 119 us (0.944)
  other arithmetic: 3.72 us -> 0 us
  local copies, waits for them, and re-layouts: 2.23 us -> 0 us
    convert_element_type x2 -> x0, other arithmetic: 3.72 us -> none  [encode(): return jnp.where(w < 0, -fourth, fourth).astype(BF16)]
    dynamic_slice x1 -> x0, local copies, waits for them, and re-layouts: 2.23 us -> none  [local(): ofac = lax.dynamic_slice_in_dim(output_factor, tp * cols, cols, 0)]
where the time goes in v3:
time: 119 us
  Pallas kernels  118 us (99%)
    pallas_call x1, Pallas kernels, local(): pl.pallas_call(functools.partial(exchange, nfs, ntp, scale), out_shape=(j...  100 us
    pallas_call x1, Pallas kernels, local(): pl.pallas_call(functools.partial(update, width), grid=(nfs,), out_shape=(...  17.5 us

profile of v3, /device:TPU:0, one launch (start us, length us, event | category | flops | bytes accessed | tf_op | source)
XLA Modules:
  0.0 118.5 jit_solution(6490754640549243340)
XLA Ops:
  0.6 100.4 %shard_map.206 = (bf16[16,128,1024]{2,1,0:T(8,128)(2,1)}, bf16[1024,2048]{1,0:T(8,128)(2,1)}, bf16[16,16,2048]{2,1,0:T(8,128)(2,1)}, f32[16,2048]{1,0:T(8,128)}) custom-call(f32[128,1024]{1,0:T(8,128)} %vw.1, f32[1024,128]{1,0:T(8,128)} %ow.1, bf16[512,1024]{1,0:T(8,128)(2,1)} %inp_in.1, bf16[512,1024]{1,0:T(8,128)(2,1)} %ocot_in.1, ...), custom_call_target="tpu_custom_call" | custom-call | tf_op jit(solution)/shard_map/pallas_call | solution.py:341
  101.0 17.5 %shard_map.207 = (bf16[2048,1024]{1,0:T(8,128)(2,1)}, bf16[1024,2048]{1,0:T(8,128)(2,1)}, f32[128,1024]{1,0:T(8,128)}, f32[1024,128]{1,0:T(8,128)}, f32[16,1024]...) custom-call(s32[1]{0:T(128)} %bitcast.fs, ...), custom_call_target="tpu_custom_call" | custom-call | tf_op jit(solution)/shard_map/pallas_call | solution.py:378
